TPU v7x, 32 devices: a whole 2x2x4 slice. The times are simulated.
32 devices in a mesh: sp: 16 (over z, y, x), tp: 2 (over core).
Axes of the slice: x: 2, y: 2, z: 4, core: 2. Of those that a mesh axis runs over, the one named last changes fastest.
Arguments:
- residual: bfloat16 [3072, 2048], P(('sp', 'tp')), may hold values from -6 to 6
- queries: bfloat16 [3072, 1024], P('sp', 'tp'), may hold values from -6 to 6
- key_pairs: bfloat16 [3072, 1024], P('sp', 'tp'), may hold values from -6 to 6
- values: bfloat16 [3072, 1024], P('sp', 'tp'), may hold values from -6 to 6
- second_weight: float32 [8], P('tp'), may hold values from 0.3 to 0.8
- head_gain: float32 [1024], P('tp'), may hold values from 0.1 to 1.9
- out_weight: bfloat16 [1024, 2048], P('tp'), may hold values from -0.1875 to 0.1875
- norm_gain: float32 [2048], replicated, may hold values from 0.1 to 1.9
- up_weight: bfloat16 [2048, 5632], P('sp', 'tp'), may hold values from -0.125 to 0.125
- gate_weight: bfloat16 [2048, 5632], P('sp', 'tp'), may hold values from -0.125 to 0.125
- conv_weight: float32 [3, 5632], P(None, 'tp'), may hold values from -3.5 to 3.5
- conv_bias: float32 [5632], P('tp'), may hold values from -3 to 3
- down_weight: bfloat16 [5632, 2048], P('tp', 'sp'), may hold values from -0.078125 to 0.078125
Outputs:
- layer_out: bfloat16 [3072, 2048], P(('sp', 'tp'))
All inputs are finite; a program needn't handle non-finite values.
Results may differ from a plain program's by a relative error of at most 0.017.
Values may be sent and summed in bfloat16 or wider, within the bound.
A program may use at most 128 MiB of HBM per device.

v0:
```python
import jax
import jax.numpy as jnp
from jax import lax
from jax.sharding import PartitionSpec as P

HD = 64
VD = 128
eps = 1e-05
neg_fill = -1e30


def from_behind(value, axis, steps):
    count = lax.axis_size(axis)
    leading, last = (max(0, -steps), min(count, count - steps))
    return lax.ppermute(value, axis, [(source, source + steps) for source in range(leading, last)])


def normalize(rows_in, gain):
    values_f = rows_in.astype(jnp.float32)
    scale_inv = lax.rsqrt(jnp.mean(values_f * values_f, axis=-1, keepdims=True) + eps)
    return (values_f * scale_inv * gain).astype(jnp.bfloat16)


def local(
    residual,
    queries,
    key_pairs,
    values,
    second_weight,
    head_gain,
    out_weight,
    norm_gain,
    up_weight,
    gate_weight,
    conv_weight,
    conv_bias,
    down_weight,
):
    tok_rows = queries.shape[0]
    head_count = second_weight.shape[0]
    ff_local = up_weight.shape[1]
    sp_index = lax.axis_index("sp")
    query = queries.reshape(tok_rows, head_count, 2, HD)
    query_pos = sp_index * tok_rows + jnp.arange(tok_rows)
    last_query = (sp_index + 1) * tok_rows
    initial = (
        jnp.full((head_count, 2, tok_rows), neg_fill, jnp.float32),
        jnp.zeros((head_count, 2, tok_rows), jnp.float32),
        jnp.zeros((head_count, 2, tok_rows, VD), jnp.float32),
    )
    key_piece = lax.all_gather(key_pairs, "sp", axis=0, tiled=True)
    value_piece = lax.all_gather(values, "sp", axis=0, tiled=True)
    piece_len = key_piece.shape[0]

    def compute(state_in):
        maxima, totals, weighted = state_in
        key_rows = key_piece.reshape(piece_len, head_count, 2, HD)
        value_rows = value_piece.reshape(piece_len, head_count, VD)
        scores = jnp.einsum(
            "qhmd,khmd->hmqk", query, key_rows, preferred_element_type=jnp.float32
        ) * HD ** (-0.5)
        visible = jnp.arange(piece_len)[None, :] <= query_pos[:, None]
        scores = jnp.where(visible, scores, neg_fill)
        new_max = jnp.maximum(maxima, jnp.max(scores, axis=-1))
        exp_scores = jnp.where(visible, jnp.exp(scores - new_max[..., None]), jnp.float32(0.0))
        totals = jnp.sum(exp_scores, axis=-1)
        weighted = jnp.einsum(
            "hmqk,khe->hmqe",
            exp_scores.astype(jnp.bfloat16),
            value_rows,
            preferred_element_type=jnp.float32,
        )
        return (new_max, totals, weighted)

    def keep_state(state_in):
        return state_in

    maxima, totals, weighted = lax.cond(jnp.int32(0) < last_query, compute, keep_state, initial)
    diff = (
        weighted[:, 0] / totals[:, 0, :, None]
        - second_weight[:, None, None] * weighted[:, 1] / totals[:, 1, :, None]
    )
    diff = jnp.transpose(diff, (1, 0, 2))
    scale_inv = lax.rsqrt(jnp.mean(diff * diff, axis=-1, keepdims=True) + eps)
    attended = (
        (diff * scale_inv * head_gain.reshape(head_count, VD) * 0.8)
        .reshape(tok_rows, head_count * VD)
        .astype(jnp.bfloat16)
    )
    proj = lax.psum_scatter(
        jnp.dot(attended, out_weight, preferred_element_type=jnp.float32).astype(jnp.bfloat16),
        "tp",
        scatter_dimension=0,
        tiled=True,
    )
    mid = (residual.astype(jnp.float32) + proj.astype(jnp.float32)).astype(jnp.bfloat16)
    normed_all = lax.all_gather(normalize(mid, norm_gain), "tp", axis=0, tiled=True)
    up_sum = jnp.dot(
        normed_all,
        lax.all_gather(up_weight, "sp", axis=0, tiled=True),
        preferred_element_type=jnp.float32,
    )
    gate_sum = jnp.dot(
        normed_all,
        lax.all_gather(gate_weight, "sp", axis=0, tiled=True),
        preferred_element_type=jnp.float32,
    )
    up_proj = up_sum.astype(jnp.bfloat16)
    gate_proj = gate_sum.astype(jnp.bfloat16)
    taps = conv_weight.shape[0]
    rim_rows = from_behind(up_proj[tok_rows - (taps - 1) :], "sp", 1)
    extended = jnp.concatenate((rim_rows, up_proj), axis=0)
    conv_out = jnp.zeros((tok_rows, ff_local), jnp.float32) + conv_bias[None, :]
    for tap in range(taps):
        conv_out = conv_out + conv_weight[tap][None, :] * extended[tap : tap + tok_rows].astype(
            jnp.float32
        )
    hidden = (jax.nn.silu(conv_out) * gate_proj.astype(jnp.float32)).astype(jnp.bfloat16)
    down_all = lax.all_gather(down_weight, "sp", axis=1, tiled=True)
    ffn_out = lax.psum_scatter(
        jnp.dot(hidden, down_all, preferred_element_type=jnp.float32).astype(jnp.bfloat16),
        "tp",
        scatter_dimension=0,
        tiled=True,
    )
    return (mid.astype(jnp.float32) + ffn_out.astype(jnp.float32)).astype(jnp.bfloat16)


def solution(mesh):
    return jax.shard_map(
        local,
        mesh=mesh,
        in_specs=(
            P(("sp", "tp"), None),
            P("sp", "tp"),
            P("sp", "tp"),
            P("sp", "tp"),
            P("tp"),
            P("tp"),
            P("tp", None),
            P(),
            P("sp", "tp"),
            P("sp", "tp"),
            P(None, "tp"),
            P("tp"),
            P("tp", "sp"),
        ),
        out_specs=P(("sp", "tp"), None),
        check_vma=False,
    )
```

profile of v0, /device:TPU:0, one launch (start us, length us, event | category | flops | bytes accessed | tf_op | source)
XLA Modules:
  0.0 705.0 jit_solution(9887044699763358971)
XLA Ops:
  6.5 0.7 all-gather.6.cloned.1.call-update
  7.3 0.7 all-gather.8.cloned.1.call-update
  8.0 0.0 reduce-scatter.3.cloned.1.call-start
  8.1 72.7 %all-gather.6.cloned.1.call-done = bf16[3072,512]{1,0:T(8,128)(2,1)} async-done(((bf16[192,512]{1,0:T(8,128)(2,1)}), bf16[3072,512]{1,0:T(8,128)(2,1)}) %all-gather.6.cloned.1.call-update) | async-done | bytes 3145744 | tf_op jit(solution)/shard_map/all_gather | solution.py:51
  80.7 69.2 %all-gather.8.cloned.1.call-done = bf16[3072,512]{1,0:T(8,128)(2,1)} async-done(((bf16[192,512]{1,0:T(8,128)(2,1)}), bf16[3072,512]{1,0:T(8,128)(2,1)}) %all-gather.8.cloned.1.call-update) | async-done | bytes 3145744 | tf_op jit(solution)/shard_map/all_gather | solution.py:52
  150.0 45.3 %conditional.1 = (f32[4,2,192]{2,1,0:T(2,128)S(1)}, f32[4,2,192,128]{3,2,1,0:T(8,128)S(1)}) conditional(s32[]{:T(128)} %convert_element_type.62, () %tuple.13, (s32[]{:T(128)}, s32[192]{0:T(256)S(1)}, bf16[192,512]{1,0:T(8,128)(2,1)}, bf16[3072,512]{1,0:T(8,128)(2,1)}, bf16[3072,512]{1,0:T(8,128)(2,1)}) %tuple.14), branch_computations={%region_0.0_spmd, %region_1.4_spmd} | conditional | flops 1873869568 | bytes 80058688 | solution.py:78
  150.0 0.4 iota_compare_fusion
  150.4 4.8 copy.26
  155.2 0.1 copy.25
  155.3 11.8 %fusion = (f32[4,2,192]{2,1,0:T(2,128)S(1)}, f32[4,2,192,3072]{3,2,1,0:T(8,128)}) fusion(pred[192,3072]{1,0:T(8,128)(4,1)S(1)} %iota_compare_fusion, bf16[192,4,2,64]{0,3,2,1:T(8,128)(2,1)S(1)} %bitcast.44, bf16[3072,4,2,64]{0,3,2,1:T(8,128)(2,1)} %bitcast.42), kind=kOutput, calls=%fused_computation.2 | convolution fusion | flops 618134016 | bytes 22812672 | tf_op jit(solution)/shard_map/cond/branch_1_fun/qhmd,khmd->hmqk/dot_general | solution.py:59
  167.1 5.5 reshape.37
  172.6 10.7 %fusion.3 = f32[4,2,192,128]{3,2,1,0:T(8,128)S(1)} fusion(f32[4,2,192,3072]{3,2,1,0:T(8,128)} %get-tuple-element.52, f32[4,2,192]{2,1,0:T(2,128)S(1)} %broadcast_maximum_fusion, pred[192,3072]{1,0:T(8,128)(4,1)S(1)} %iota_compare_fusion, bf16[3072,4,128,1]{2,1,0,3:T(4,128)(2,1)} %bitcast.43), kind=kOutput, calls=%fused_computation.5 | convolution fusion | flops 1231552512 | bytes 23402496 | tf_op jit(solution)/shard_map/cond/branch_1_fun/hmqk,khe->hmqe/dot_general | solution.py:67
  183.3 11.9 %fusion.2 = f32[4,2,192]{2,1,0:T(2,128)S(1)} fusion(f32[4,2,192,3072]{3,2,1,0:T(8,128)} %get-tuple-element.52, f32[4,2,192]{2,1,0:T(2,128)S(1)} %broadcast_maximum_fusion, pred[192,3072]{1,0:T(8,128)(4,1)S(1)} %iota_compare_fusion), kind=kLoop, calls=%fused_computation.4 | loop fusion | flops 23591424 | bytes 19476480 | tf_op jit(solution)/shard_map/cond/branch_1_fun/reduce_sum | solution.py:66
  195.3 0.5 multiply_reduce_fusion
  195.8 1.5 convolution_convert_fusion.3
  197.4 0.0 all-gather.10.cloned.1.call-start
  197.4 0.5 all-gather.10.cloned.1.call-update
  198.0 0.5 all-gather.12.cloned.1.call-update
  198.6 0.5 all-gather.14.cloned.1.call-update
  199.1 5.1 reduce-scatter.3.cloned.1.call-done
  204.2 1.2 fusion.20
  205.5 1.2 fusion.22
  206.6 2.4 all_gather.20
  209.0 140.4 %all-gather.10.cloned.1.call-done = bf16[2048,2816]{1,0:T(8,128)(2,1)} async-done(((bf16[128,2816]{1,0:T(8,128)(2,1)}), bf16[2048,2816]{1,0:T(8,128)(2,1)}) %all-gather.10.cloned.1.call-update) | async-done | bytes 11534352 | tf_op jit(solution)/shard_map/all_gather | solution.py:100
  349.4 6.7 convolution_convert_fusion.1
  356.1 3.4 collective-permute-start
  359.5 0.1 slice_reduce_fusion.2
  359.6 132.0 %all-gather.12.cloned.1.call-done = bf16[2048,2816]{1,0:T(8,128)(2,1)} async-done(((bf16[128,2816]{1,0:T(8,128)(2,1)}), bf16[2048,2816]{1,0:T(8,128)(2,1)}) %all-gather.12.cloned.1.call-update) | async-done | bytes 11534352 | tf_op jit(solution)/shard_map/all_gather | solution.py:105
  491.6 182.8 %all-gather.14.cloned.1.call-done = bf16[2816,2048]{1,0:T(8,128)(2,1)} async-done(((bf16[2816,128]{1,0:T(8,128)(2,1)}), bf16[2816,2048]{1,0:T(8,128)(2,1)}) %all-gather.14.cloned.1.call-update) | async-done | bytes 11534352 | tf_op jit(solution)/shard_map/all_gather | solution.py:119
  674.5 15.2 %convolution_convert_fusion.2 = bf16[192,2048]{1,0:T(8,128)(2,1)} fusion(bf16[2816,2048]{1,0:T(8,128)(2,1)} %all-gather.14.cloned.1.call-done, bf16[192,2048]{1,0:T(8,128)(2,1)} %copy-done.4, bf16[2048,2816]{1,0:T(8,128)(2,1)} %all-gather.12.cloned.1.call-done, bf16[192,2816]{1,0:T(8,128)(2,1)} %copy-done.10, bf16[2,2816]{1,0:T(2,128)(2,1)S(1)} %collective-permute-done, ...), kind=kOutput, calls=%fused_computation.19 | convolution fusion | flops 4442013696 | bytes 25779200 | tf_op jit(solution)/shard_map/dot_general | solution.py:121
  689.7 6.5 reduce-scatter.5.cloned.1.call-done
  696.2 1.9 fusion.23
  (40 shorter events, 0.3 us)
Async XLA Ops:
  6.5 189.2 %copy-start = (bf16[512,2048]{1,0:T(8,128)(2,1)S(1)}, bf16[512,2048]{1,0:T(8,128)(2,1)}, u32[]{:S(2)}) copy-start(bf16[512,2048]{1,0:T(8,128)(2,1)} %param.21) | copy-start | bytes 6291460
  6.5 74.2 %all-gather.6.cloned.1.call-start = ((), (), s32[]{:S(2)}) async-start(), calls=%async_computation.2 | async-start | bytes 3342336 | tf_op jit(solution)/shard_map/all_gather | solution.py:51
  7.3 142.7 %all-gather.8.cloned.1.call-start = ((), (), s32[]{:S(2)}) async-start(), calls=%async_computation.3 | async-start | bytes 3342336 | tf_op jit(solution)/shard_map/all_gather | solution.py:52
  8.0 196.2 %reduce-scatter.3.cloned.1.call-start = ((), (), s32[]{:S(2)}) async-start(), calls=%async_computation.4 | async-start | bytes 1179648 | tf_op jit(solution)/shard_map/reduce_scatter | solution.py:90
  149.9 45.3 %copy-start.9 = (f32[4]{0:T(128)S(1)}, f32[4]{0:T(128)}, u32[]{:S(2)}) copy-start(f32[4]{0:T(128)} %param.19) | copy-start | bytes 52
  149.9 45.8 %copy-start.8 = (f32[512]{0:T(512)S(1)}, f32[512]{0:T(512)}, u32[]{:S(2)}) copy-start(f32[512]{0:T(512)} %param.20) | copy-start | bytes 6148
  150.3 4.8 copy-start.5
  195.7 8.5 %copy-start.2 = (bf16[96,2048]{1,0:T(8,128)(2,1)S(1)}, bf16[96,2048]{1,0:T(8,128)(2,1)}, u32[]{:S(2)}) copy-start(bf16[96,2048]{1,0:T(8,128)(2,1)} %param.15) | copy-start | bytes 1179652
  195.8 9.7 %copy-start.7 = (f32[2048]{0:T(1024)S(1)}, f32[2048]{0:T(1024)}, u32[]{:S(2)}) copy-start(f32[2048]{0:T(1024)} %param.22) | copy-start | bytes 24580
  197.4 152.0 %all-gather.10.cloned.1.call-start = ((), (), s32[]{:S(2)}) async-start(), calls=%async_computation.5 | async-start | bytes 12255232 | tf_op jit(solution)/shard_map/all_gather | solution.py:100
  197.9 293.7 %all-gather.12.cloned.1.call-start = ((), (), s32[]{:S(2)}) async-start(), calls=%async_computation.6 | async-start | bytes 12255232 | tf_op jit(solution)/shard_map/all_gather | solution.py:105
  198.5 475.9 %all-gather.14.cloned.1.call-start = ((), (), s32[]{:S(2)}) async-start(), calls=%async_computation.7 | async-start | bytes 12255232 | tf_op jit(solution)/shard_map/all_gather | solution.py:119
  199.1 497.1 %reduce-scatter.5.cloned.1.call-start = ((), (), s32[]{:S(2)}) async-start(), calls=%async_computation.8 | async-start | bytes 1179648 | tf_op jit(solution)/shard_map/reduce_scatter | solution.py:120
  209.0 147.1 %copy-start.4 = (bf16[192,2048]{1,0:T(8,128)(2,1)}, bf16[192,2048]{1,0:T(8,128)(2,1)S(1)}, u32[]{:S(2)}) copy-start(bf16[192,2048]{1,0:T(8,128)(2,1)S(1)} %all_gather.20) | copy-start | bytes 2359300
  209.0 150.5 %copy-start.6 = (f32[3,2816]{1,0:T(4,128)S(1)}, f32[3,2816]{1,0:T(4,128)}, u32[]{:S(2)}) copy-start(f32[3,2816]{1,0:T(4,128)} %param.25) | copy-start | bytes 101380
  209.0 465.5 %copy-start.11 = (f32[2816]{0:T(1024)S(1)}, f32[2816]{0:T(1024)}, u32[]{:S(2)}) copy-start(f32[2816]{0:T(1024)} %param.26) | copy-start | bytes 33796
  356.1 3.4 copy-start.10
  356.1 318.3 %collective-permute-start = (bf16[2,2816]{1,0:T(2,128)(2,1)S(1)}, bf16[2,2816]{1,0:T(2,128)(2,1)S(1)}, u32[]{:S(2)}, u32[]{:S(2)}) collective-permute-start(bf16[2,2816]{1,0:T(2,128)(2,1)S(1)} %slice.41), channel_id=1, source_target_pairs={{0,2},{2,4},{4,6},{6,8},{8,10},{10,12},{12,14},{14,16},{16,18},{18... | collective-permute-start | bytes 33800 | tf_op jit(solution)/shard_map/ppermute | solution.py:15
  674.5 21.8 %copy-start.3 = (bf16[96,2048]{1,0:T(8,128)(2,1)S(1)}, bf16[96,2048]{1,0:T(8,128)(2,1)}, u32[]{:S(2)}) copy-start(bf16[96,2048]{1,0:T(8,128)(2,1)} %reduce-scatter.3.cloned.1.call-done) | copy-start | bytes 1179652
  674.5 23.7 %copy-start.1 = (bf16[512,2048]{1,0:T(8,128)(2,1)S(1)}, bf16[512,2048]{1,0:T(8,128)(2,1)}, u32[]{:S(2)}) copy-start(bf16[512,2048]{1,0:T(8,128)(2,1)} %param.21) | copy-start | bytes 6291460
Sparse Core Ops, SparseCore 0:
  10.1 70.5 all-gather.5
  83.5 66.3 all-gather.7
  197.5 6.6 reduce-scatter.2
  206.8 142.5 all-gather.9
  352.0 139.5 all-gather.11
  494.2 180.2 all-gather.13
  689.8 6.3 reduce-scatter.4
where the time goes:
time: 706 us; the launch traced here: 705 us
  waiting for transfers between devices  612 us (87%)
  matrix products  45.9 us (7%)
  other arithmetic  17.1 us (2%)
  between operations  13.6 us (2%)
  local copies, waits for them, and re-layouts  10.6 us (2%)
    all_gather x1, waiting for transfers between devices, local(): down_all = lax.all_gather(down_weight, 'sp', axis=1, tiled=True)  183 us
    all_gather x1, waiting for transfers between devices, local(): lax.all_gather(up_weight, 'sp', axis=0, tiled=True)  140 us
    all_gather x1, waiting for transfers between devices, local(): lax.all_gather(gate_weight, 'sp', axis=0, tiled=True)  132 us
    all_gather x1, waiting for transfers between devices, local(): key_piece = lax.all_gather(key_pairs, 'sp', axis=0, tiled=True)  72.7 us
    all_gather x1, waiting for transfers between devices, local(): value_piece = lax.all_gather(values, 'sp', axis=0, tiled=True)  69.2 us
    dot_general x1, matrix products, local(): jnp.dot(hidden, down_all, preferred_element_type=jnp.float32)  15.2 us
  transfers between devices with their start and end apart: 8, of which 7 were waited for; matrix products, arithmetic and copies ran while one was open for 1% of the time, Pallas kernels for 0%

commit v1 on v0

--- a/solution.py
+++ b/solution.py
@@ -116,7 +116,7 @@
             jnp.float32
         )
     hidden = (jax.nn.silu(conv_out) * gate_proj.astype(jnp.float32)).astype(jnp.bfloat16)
-    down_all = lax.all_gather(down_weight, "sp", axis=1, tiled=True)
+    down_all = jnp.concatenate(lax.all_gather(down_weight, axis_name="sp"), axis=1)
     ffn_out = lax.psum_scatter(
         jnp.dot(hidden, down_all, preferred_element_type=jnp.float32).astype(jnp.bfloat16),
         "tp",

time: 706 us -> 666 us (0.943)
  waiting for transfers between devices: 612 us -> 556 us
  local copies, waits for them, and re-layouts: 10.6 us -> 25.8 us
    all_gather x1, waiting for transfers between devices: 183 us -> 132 us  [local(): lax.all_gather(down_weight, axis_name='sp')]
    reshape x0 -> x1, local copies, waits for them, and re-layouts: none -> 15.2 us  [local(): jnp.concatenate(lax.all_gather(down_weight, axis_name='sp'), axis=1)]
  transfers between devices with their start and end apart: 8 -> 8, of which waited for: 7 -> 7; matrix products, arithmetic and copies ran while one was open for 1% -> 4% of each run, Pallas kernels for 0% -> 0%
where the time goes in v1:
time: 666 us; the launch traced here: 665 us
  waiting for transfers between devices  556 us (83%)
  matrix products  46.5 us (7%)
  local copies, waits for them, and re-layouts  25.8 us (4%)
  other arithmetic  17.1 us (3%)
  between operations  13.6 us (2%)
    all_gather x1, waiting for transfers between devices, local(): lax.all_gather(up_weight, 'sp', axis=0, tiled=True)  140 us
    all_gather x1, waiting for transfers between devices, local(): lax.all_gather(down_weight, axis_name='sp')  132 us
    all_gather x1, waiting for transfers between devices, local(): lax.all_gather(gate_weight, 'sp', axis=0, tiled=True)  127 us
    all_gather x1, waiting for transfers between devices, local(): key_piece = lax.all_gather(key_pairs, 'sp', axis=0, tiled=True)  72.7 us
    all_gather x1, waiting for transfers between devices, local(): value_piece = lax.all_gather(values, 'sp', axis=0, tiled=True)  69.2 us
    dot_general x1, matrix products, local(): jnp.dot(hidden, down_all, preferred_element_type=jnp.float32)  15.8 us
    reshape x1, local copies, waits for them, and re-layouts, local(): jnp.concatenate(lax.all_gather(down_weight, axis_name='sp'), axis=1)  15.2 us
  transfers between devices with their start and end apart: 8, of which 7 were waited for; matrix products, arithmetic and copies ran while one was open for 4% of the time, Pallas kernels for 0%

profile of v1, /device:TPU:0, one launch (start us, length us, event | category | flops | bytes accessed | tf_op | source)
XLA Modules:
  0.0 665.0 jit_solution(90706076767632462)
XLA Ops:
  6.5 0.7 all-gather.7.cloned.1.call-update
  7.3 0.7 all-gather.9.cloned.1.call-update
  8.1 72.7 %all-gather.7.cloned.1.call-done = bf16[3072,512]{1,0:T(8,128)(2,1)} async-done(((bf16[192,512]{1,0:T(8,128)(2,1)}), bf16[3072,512]{1,0:T(8,128)(2,1)}) %all-gather.7.cloned.1.call-update) | async-done | bytes 3145744 | tf_op jit(solution)/shard_map/all_gather | solution.py:51
  80.7 69.2 %all-gather.9.cloned.1.call-done = bf16[3072,512]{1,0:T(8,128)(2,1)} async-done(((bf16[192,512]{1,0:T(8,128)(2,1)}), bf16[3072,512]{1,0:T(8,128)(2,1)}) %all-gather.9.cloned.1.call-update) | async-done | bytes 3145744 | tf_op jit(solution)/shard_map/all_gather | solution.py:52
  150.0 45.3 %conditional.1 = (f32[4,2,192]{2,1,0:T(2,128)S(1)}, f32[4,2,192,128]{3,2,1,0:T(8,128)S(1)}) conditional(s32[]{:T(128)} %convert_element_type.62, () %tuple.13, (s32[]{:T(128)}, s32[192]{0:T(256)S(1)}, bf16[192,512]{1,0:T(8,128)(2,1)}, bf16[3072,512]{1,0:T(8,128)(2,1)}, bf16[3072,512]{1,0:T(8,128)(2,1)}) %tuple.14), branch_computations={%region_0.0_spmd, %region_1.4_spmd} | conditional | flops 1873869568 | bytes 80058688 | solution.py:78
  150.0 0.4 iota_compare_fusion
  150.4 4.8 copy.32
  155.2 0.1 copy.31
  155.3 11.8 %fusion = (f32[4,2,192]{2,1,0:T(2,128)S(1)}, f32[4,2,192,3072]{3,2,1,0:T(8,128)}) fusion(pred[192,3072]{1,0:T(8,128)(4,1)S(1)} %iota_compare_fusion, bf16[192,4,2,64]{0,3,2,1:T(8,128)(2,1)S(1)} %bitcast.50, bf16[3072,4,2,64]{0,3,2,1:T(8,128)(2,1)} %bitcast.46), kind=kOutput, calls=%fused_computation.2 | convolution fusion | flops 618134016 | bytes 22812672 | tf_op jit(solution)/shard_map/cond/branch_1_fun/qhmd,khmd->hmqk/dot_general | solution.py:59
  167.1 5.5 reshape.41
  172.6 10.7 %fusion.3 = f32[4,2,192,128]{3,2,1,0:T(8,128)S(1)} fusion(f32[4,2,192,3072]{3,2,1,0:T(8,128)} %get-tuple-element.57, f32[4,2,192]{2,1,0:T(2,128)S(1)} %broadcast_maximum_fusion, pred[192,3072]{1,0:T(8,128)(4,1)S(1)} %iota_compare_fusion, bf16[3072,4,128,1]{2,1,0,3:T(4,128)(2,1)} %bitcast.49), kind=kOutput, calls=%fused_computation.5 | convolution fusion | flops 1231552512 | bytes 23402496 | tf_op jit(solution)/shard_map/cond/branch_1_fun/hmqk,khe->hmqe/dot_general | solution.py:67
  183.3 11.9 %fusion.2 = f32[4,2,192]{2,1,0:T(2,128)S(1)} fusion(f32[4,2,192,3072]{3,2,1,0:T(8,128)} %get-tuple-element.57, f32[4,2,192]{2,1,0:T(2,128)S(1)} %broadcast_maximum_fusion, pred[192,3072]{1,0:T(8,128)(4,1)S(1)} %iota_compare_fusion), kind=kLoop, calls=%fused_computation.4 | loop fusion | flops 23591424 | bytes 19476480 | tf_op jit(solution)/shard_map/cond/branch_1_fun/reduce_sum | solution.py:66
  195.3 0.5 multiply_reduce_fusion
  195.8 1.5 convolution_convert_fusion.3
  197.4 0.0 all-gather.11.cloned.1.call-start
  197.4 0.5 all-gather.11.cloned.1.call-update
  198.0 0.5 all-gather.15.cloned.1.call-update
  198.6 0.5 all-gather.13.cloned.1.call-update
  199.1 5.1 reduce-scatter.3.cloned.1.call-done
  204.2 1.2 fusion.20
  205.5 1.2 fusion.22
  206.6 2.4 all_gather.23
  209.0 140.4 %all-gather.11.cloned.1.call-done = bf16[2048,2816]{1,0:T(8,128)(2,1)} async-done(((bf16[128,2816]{1,0:T(8,128)(2,1)}), bf16[2048,2816]{1,0:T(8,128)(2,1)}) %all-gather.11.cloned.1.call-update) | async-done | bytes 11534352 | tf_op jit(solution)/shard_map/all_gather | solution.py:100
  349.4 6.7 %convolution_convert_fusion.1 = bf16[192,2816]{1,0:T(8,128)(2,1)S(1)} fusion(bf16[192,2048]{1,0:T(8,128)(2,1)S(1)} %all_gather.23, bf16[2048,2816]{1,0:T(8,128)(2,1)} %all-gather.11.cloned.1.call-done), kind=kOutput, calls=%fused_computation.17 | convolution fusion | flops 2215133184 | bytes 13402112 | tf_op jit(solution)/shard_map/dot_general | solution.py:98
  356.1 3.2 collective-permute-start
  359.3 0.1 slice_reduce_fusion.2
  359.4 132.2 %all-gather.15.cloned.1.call-done = bf16[45056,128]{1,0:T(8,128)(2,1)} async-done(((bf16[2816,128]{1,0:T(8,128)(2,1)}), bf16[45056,128]{1,0:T(8,128)(2,1)}) %all-gather.15.cloned.1.call-update) | async-done | bytes 11534352 | tf_op jit(solution)/shard_map/all_gather | solution.py:119
  491.6 15.2 %copy.35 = bf16[2816,16,128]{0,2,1:T(8,128)(2,1)} copy(bf16[2816,16,128]{2,0,1:T(8,128)(2,1)} %bitcast.47) | data formatting | bytes 23068672 | tf_op jit(solution)/shard_map/reshape | solution.py:119
  506.8 127.0 %all-gather.13.cloned.1.call-done = bf16[2048,2816]{1,0:T(8,128)(2,1)} async-done(((bf16[128,2816]{1,0:T(8,128)(2,1)}), bf16[2048,2816]{1,0:T(8,128)(2,1)}) %all-gather.13.cloned.1.call-update) | async-done | bytes 11534352 | tf_op jit(solution)/shard_map/all_gather | solution.py:105
  633.9 15.8 %convolution_convert_fusion.2 = bf16[192,2048]{1,0:T(8,128)(2,1)} fusion(bf16[2816,2048]{0,1:T(8,128)(2,1)} %bitcast.48, bf16[192,2048]{1,0:T(8,128)(2,1)} %copy-done.4, bf16[2048,2816]{1,0:T(8,128)(2,1)} %all-gather.13.cloned.1.call-done, bf16[192,2816]{1,0:T(8,128)(2,1)} %copy-done.10, bf16[2,2816]{1,0:T(2,128)(2,1)S(1)} %collective-permute-done, ...), kind=kOutput, calls=%fused_computation.19 | convolution fusion | flops 4442013696 | bytes 25779200 | tf_op jit(solution)/shard_map/dot_general | solution.py:121
  649.8 6.5 reduce-scatter.5.cloned.1.call-done
  656.3 1.9 fusion.23
  (41 shorter events, 0.3 us)
Async XLA Ops:
  6.5 189.2 %copy-start = (bf16[512,2048]{1,0:T(8,128)(2,1)S(1)}, bf16[512,2048]{1,0:T(8,128)(2,1)}, u32[]{:S(2)}) copy-start(bf16[512,2048]{1,0:T(8,128)(2,1)} %param.21) | copy-start | bytes 6291460
  6.5 74.2 %all-gather.7.cloned.1.call-start = ((), (), s32[]{:S(2)}) async-start(), calls=%async_computation.2 | async-start | bytes 3342336 | tf_op jit(solution)/shard_map/all_gather | solution.py:51
  7.3 142.7 %all-gather.9.cloned.1.call-start = ((), (), s32[]{:S(2)}) async-start(), calls=%async_computation.3 | async-start | bytes 3342336 | tf_op jit(solution)/shard_map/all_gather | solution.py:52
  8.0 196.2 %reduce-scatter.3.cloned.1.call-start = ((), (), s32[]{:S(2)}) async-start(), calls=%async_computation.4 | async-start | bytes 1179648 | tf_op jit(solution)/shard_map/reduce_scatter | solution.py:90
  149.9 45.3 %copy-start.9 = (f32[4]{0:T(128)S(1)}, f32[4]{0:T(128)}, u32[]{:S(2)}) copy-start(f32[4]{0:T(128)} %param.19) | copy-start | bytes 52
  149.9 45.8 %copy-start.8 = (f32[512]{0:T(512)S(1)}, f32[512]{0:T(512)}, u32[]{:S(2)}) copy-start(f32[512]{0:T(512)} %param.20) | copy-start | bytes 6148
  150.3 4.8 copy-start.5
  195.7 8.5 %copy-start.2 = (bf16[96,2048]{1,0:T(8,128)(2,1)S(1)}, bf16[96,2048]{1,0:T(8,128)(2,1)}, u32[]{:S(2)}) copy-start(bf16[96,2048]{1,0:T(8,128)(2,1)} %param.15) | copy-start | bytes 1179652
  195.8 9.7 %copy-start.7 = (f32[2048]{0:T(1024)S(1)}, f32[2048]{0:T(1024)}, u32[]{:S(2)}) copy-start(f32[2048]{0:T(1024)} %param.22) | copy-start | bytes 24580
  197.4 152.0 %all-gather.11.cloned.1.call-start = ((), (), s32[]{:S(2)}) async-start(), calls=%async_computation.5 | async-start | bytes 12255232 | tf_op jit(solution)/shard_map/all_gather | solution.py:100
  197.9 293.7 %all-gather.15.cloned.1.call-start = ((), (), s32[]{:S(2)}) async-start(), calls=%async_computation.8 | async-start | bytes 12255232 | tf_op jit(solution)/shard_map/all_gather | solution.py:119
  198.5 435.4 %all-gather.13.cloned.1.call-start = ((), (), s32[]{:S(2)}) async-start(), calls=%async_computation.6 | async-start | bytes 12255232 | tf_op jit(solution)/shard_map/all_gather | solution.py:105
  199.1 457.1 %reduce-scatter.5.cloned.1.call-start = ((), (), s32[]{:S(2)}) async-start(), calls=%async_computation.7 | async-start | bytes 1179648 | tf_op jit(solution)/shard_map/reduce_scatter | solution.py:120
  209.0 147.1 %copy-start.4 = (bf16[192,2048]{1,0:T(8,128)(2,1)}, bf16[192,2048]{1,0:T(8,128)(2,1)S(1)}, u32[]{:S(2)}) copy-start(bf16[192,2048]{1,0:T(8,128)(2,1)S(1)} %all_gather.23) | copy-start | bytes 2359300
  209.0 150.3 %copy-start.6 = (f32[3,2816]{1,0:T(4,128)S(1)}, f32[3,2816]{1,0:T(4,128)}, u32[]{:S(2)}) copy-start(f32[3,2816]{1,0:T(4,128)} %param.25) | copy-start | bytes 101380
  356.1 3.2 copy-start.10
  356.1 277.8 %collective-permute-start = (bf16[2,2816]{1,0:T(2,128)(2,1)S(1)}, bf16[2,2816]{1,0:T(2,128)(2,1)S(1)}, u32[]{:S(2)}, u32[]{:S(2)}) collective-permute-start(bf16[2,2816]{1,0:T(2,128)(2,1)S(1)} %slice.41), channel_id=1, source_target_pairs={{0,2},{2,4},{4,6},{6,8},{8,10},{10,12},{12,14},{14,16},{16,18},{18... | collective-permute-start | bytes 33800 | tf_op jit(solution)/shard_map/ppermute | solution.py:15
  491.6 142.3 %copy-start.11 = (f32[2816]{0:T(1024)S(1)}, f32[2816]{0:T(1024)}, u32[]{:S(2)}) copy-start(f32[2816]{0:T(1024)} %param.26) | copy-start | bytes 33796
  633.9 22.4 %copy-start.3 = (bf16[96,2048]{1,0:T(8,128)(2,1)S(1)}, bf16[96,2048]{1,0:T(8,128)(2,1)}, u32[]{:S(2)}) copy-start(bf16[96,2048]{1,0:T(8,128)(2,1)} %reduce-scatter.3.cloned.1.call-done) | copy-start | bytes 1179652
  633.9 24.3 %copy-start.1 = (bf16[512,2048]{1,0:T(8,128)(2,1)S(1)}, bf16[512,2048]{1,0:T(8,128)(2,1)}, u32[]{:S(2)}) copy-start(bf16[512,2048]{1,0:T(8,128)(2,1)} %param.21) | copy-start | bytes 6291460
Sparse Core Ops, SparseCore 0:
  10.1 70.5 all-gather.6
  83.5 66.3 all-gather.8
  197.5 6.6 reduce-scatter.2
  206.8 142.5 all-gather.10
  352.0 139.5 all-gather.14
  494.2 139.5 all-gather.12
  649.9 6.3 reduce-scatter.4
